TPU v7x, 32 devices: a whole 2x2x4 slice. The times are simulated.
32 devices in a mesh: fs: 16 (over z, y, x), tp: 2 (over core).
Axes of the slice: x: 2, y: 2, z: 4, core: 2. Of those that a mesh axis runs over, the one named last changes fastest.
Arguments:
- tokens: bfloat16 [6144, 2048], P('fs'), may hold values from -6 to 6
- merged: bfloat16 [6144, 2048], P('fs'), may hold values from -6 to 6
- gain_first: float32 [2048], replicated, may hold values from 0.1 to 1.9
- gate_first: bfloat16 [2048, 2816], P('fs', 'tp'), may hold values from -0.125 to 0.125
- up_first: bfloat16 [2048, 2816], P('fs', 'tp'), may hold values from -0.125 to 0.125
- down_first: bfloat16 [2816, 2048], P('tp', 'fs'), may hold values from -0.21875 to 0.21875
- gain_second: float32 [2048], replicated, may hold values from 0.1 to 1.9
- gate_second: bfloat16 [2048, 2816], P('fs', 'tp'), may hold values from -0.125 to 0.125
- up_second: bfloat16 [2048, 2816], P('fs', 'tp'), may hold values from -0.125 to 0.125
- down_second: bfloat16 [2816, 2048], P('tp', 'fs'), may hold values from -0.21875 to 0.21875
Outputs:
- result: bfloat16 [6144, 2048], P('fs')
All inputs are finite; a program needn't handle non-finite values.
Results may differ from a plain program's by a relative error of at most 0.01.
Values may be sent and summed in bfloat16 or wider, within the bound.
A program may use at most 64 MiB of HBM per device.

v0:
```python
import jax
import jax.numpy as jnp
from jax import lax
from jax.sharding import PartitionSpec as P

EPS = 1e-06


def norm_rows(values, gain):
    scale = lax.rsqrt(jnp.mean(values * values, axis=-1, keepdims=True) + EPS)
    return values * scale * gain


def make_folder(normed, pieces):
    return (
        jnp.dot(normed, pieces[0], preferred_element_type=jnp.float32),
        jnp.dot(normed, pieces[1], preferred_element_type=jnp.float32),
    )


def shards(
    tokens,
    merged,
    gain_first,
    gate_first,
    up_first,
    down_first,
    gain_second,
    gate_second,
    up_second,
    down_second,
):
    normed_first = norm_rows(tokens.astype(jnp.float32), gain_first).astype(jnp.bfloat16)
    gate, up = make_folder(
        normed_first,
        (
            lax.all_gather(gate_first, "fs", axis=0, tiled=True),
            lax.all_gather(up_first, "fs", axis=0, tiled=True),
        ),
    )
    hidden = (jax.nn.silu(gate) * up).astype(jnp.bfloat16)
    down_whole = lax.all_gather(down_first, "fs", axis=1, tiled=True)
    partial_value = jnp.dot(hidden, down_whole, preferred_element_type=jnp.float32)
    first_sum = lax.psum(partial_value.astype(jnp.bfloat16), "tp").astype(jnp.float32)
    middle = tokens.astype(jnp.float32) + merged.astype(jnp.float32) + 0.5 * first_sum
    normed_second = norm_rows(middle, gain_second).astype(jnp.bfloat16)
    gate_two, up_two = make_folder(
        normed_second,
        (
            lax.all_gather(gate_second, "fs", axis=0, tiled=True),
            lax.all_gather(up_second, "fs", axis=0, tiled=True),
        ),
    )
    hidden_two = (jax.nn.silu(gate_two) * up_two).astype(jnp.bfloat16)
    down_two = lax.all_gather(down_second, "fs", axis=1, tiled=True)
    partial_two = jnp.dot(hidden_two, down_two, preferred_element_type=jnp.float32)
    second_sum = lax.psum(partial_two.astype(jnp.bfloat16), "tp").astype(jnp.float32)
    return (middle + 0.5 * second_sum).astype(jnp.bfloat16)


def solution(mesh):
    return jax.shard_map(
        shards,
        mesh=mesh,
        in_specs=(
            P("fs", None),
            P("fs", None),
            P(),
            P("fs", "tp"),
            P("fs", "tp"),
            P("tp", "fs"),
            P(),
            P("fs", "tp"),
            P("fs", "tp"),
            P("tp", "fs"),
        ),
        out_specs=P("fs", None),
        check_vma=False,
    )
```

profile of v0, /device:TPU:0, one launch (start us, length us, event | category | flops | bytes accessed | tf_op | source)
XLA Modules:
  0.0 665.2 jit_solution(4083028435205835512)
XLA Ops:
  6.5 0.0 all-gather.7.cloned.1.call-start
  6.5 0.7 all-gather.7.cloned.1.call-update
  7.3 0.0 all-gather.11.cloned.1.call-start
  7.3 0.7 all-gather.11.cloned.1.call-update
  8.0 0.0 all-gather.9.cloned.1.call-start
  8.1 0.7 all-gather.9.cloned.1.call-update
  8.7 0.0 all-reduce.3.cloned.1.call-start
  8.8 1.8 fusion.1
  10.6 0.0 copy-start
  10.6 0.0 copy-start.4
  10.6 90.9 %all-gather.7.cloned.1.call-done = bf16[2048,1408]{1,0:T(8,128)(2,1)} async-done(((bf16[128,1408]{1,0:T(8,128)(2,1)}), bf16[2048,1408]{1,0:T(8,128)(2,1)}) %all-gather.7.cloned.1.call-update) | async-done | bytes 5767184 | tf_op jit(solution)/shard_map/all_gather | solution.py:37
  101.5 7.1 %fusion.8 = f32[384,1408]{1,0:T(8,128)} fusion(bf16[2048,1408]{1,0:T(8,128)(2,1)} %all-gather.7.cloned.1.call-done, bf16[384,2048]{1,0:T(8,128)(2,1)} %param.10, f32[2048]{0:T(1024)} %param.12, f32[384]{0:T(512)S(1)} %add_rsqrt_fusion.1), kind=kOutput, calls=%fused_computation.16 | convolution fusion | flops 2217738240 | bytes 9512448 | tf_op jit(solution)/shard_map/dot_general | solution.py:16
  108.7 102.6 %all-gather.11.cloned.1.call-done = bf16[1408,2048]{1,0:T(8,128)(2,1)} async-done(((bf16[1408,128]{1,0:T(8,128)(2,1)}), bf16[1408,2048]{1,0:T(8,128)(2,1)}) %all-gather.11.cloned.1.call-update) | async-done | bytes 5767184 | tf_op jit(solution)/shard_map/all_gather | solution.py:42
  211.3 89.7 %all-gather.9.cloned.1.call-done = bf16[2048,1408]{1,0:T(8,128)(2,1)} async-done(((bf16[128,1408]{1,0:T(8,128)(2,1)}), bf16[2048,1408]{1,0:T(8,128)(2,1)}) %all-gather.9.cloned.1.call-update) | async-done | bytes 5767184 | tf_op jit(solution)/shard_map/all_gather | solution.py:38
  300.9 0.0 copy-done
  300.9 0.0 copy-done.4
  300.9 11.2 %convolution_convert_fusion.1 = bf16[384,2048]{1,0:T(8,128)(2,1)} fusion(bf16[1408,2048]{1,0:T(8,128)(2,1)} %all-gather.11.cloned.1.call-done, bf16[2048,1408]{1,0:T(8,128)(2,1)} %all-gather.9.cloned.1.call-done, f32[384,1408]{1,0:T(8,128)} %fusion.8, bf16[384,2048]{1,0:T(8,128)(2,1)S(1)} %copy-done, f32[2048]{0:T(1024)S(1)} %copy-done.4, ...), kind=kOutput, calls=%fused_computation.15 | convolution fusion | flops 4436361216 | bytes 16852480 | tf_op jit(solution)/shard_map/dot_general | solution.py:43
  312.1 0.0 copy-start.1
  312.1 0.0 all-reduce.3.cloned.1.call-update
  312.2 0.0 copy-start.3
  312.2 0.0 all-gather.13.cloned.1.call-start
  312.2 0.5 all-gather.13.cloned.1.call-update
  312.8 0.0 all-gather.15.cloned.1.call-start
  312.8 0.5 all-gather.15.cloned.1.call-update
  313.3 0.0 all-gather.17.cloned.1.call-start
  313.4 0.7 all-gather.17.cloned.1.call-update
  314.1 0.2 all-reduce.5.cloned.1.call-start
  314.3 17.0 %all-reduce.3.cloned.1.call-done = bf16[384,2048]{1,0:T(8,128)(2,1)} async-done(((bf16[384,2048]{1,0:T(8,128)(2,1)}), bf16[384,2048]{1,0:T(8,128)(2,1)}) %all-reduce.3.cloned.1.call-update) | async-done | bytes 1572880 | tf_op jit(solution)/shard_map/psum | solution.py:44
  331.3 0.0 copy-done.1
  331.3 0.0 copy-start.2
  331.3 2.4 multiply_reduce_fusion
  333.8 0.0 copy-done.3
  333.8 0.0 copy-done.2
  333.8 2.2 multiply_convert_fusion
  336.0 87.8 %all-gather.13.cloned.1.call-done = bf16[2048,1408]{1,0:T(8,128)(2,1)} async-done(((bf16[128,1408]{1,0:T(8,128)(2,1)}), bf16[2048,1408]{1,0:T(8,128)(2,1)}) %all-gather.13.cloned.1.call-update) | async-done | bytes 5767184 | tf_op jit(solution)/shard_map/all_gather | solution.py:50
  423.8 7.1 %fusion.12 = f32[384,1408]{1,0:T(8,128)} fusion(bf16[384,2048]{1,0:T(8,128)(2,1)} %multiply_convert_fusion, bf16[2048,1408]{1,0:T(8,128)(2,1)} %all-gather.13.cloned.1.call-done), kind=kOutput, calls=%fused_computation.21 | convolution fusion | flops 2214592512 | bytes 9502720 | tf_op jit(solution)/shard_map/dot_general | solution.py:16
  430.9 82.9 %all-gather.15.cloned.1.call-done = bf16[2048,1408]{1,0:T(8,128)(2,1)} async-done(((bf16[128,1408]{1,0:T(8,128)(2,1)}), bf16[2048,1408]{1,0:T(8,128)(2,1)}) %all-gather.15.cloned.1.call-update) | async-done | bytes 5767184 | tf_op jit(solution)/shard_map/all_gather | solution.py:51
  513.8 109.7 %all-gather.17.cloned.1.call-done = bf16[1408,2048]{1,0:T(8,128)(2,1)} async-done(((bf16[1408,128]{1,0:T(8,128)(2,1)}), bf16[1408,2048]{1,0:T(8,128)(2,1)}) %all-gather.17.cloned.1.call-update) | async-done | bytes 5767184 | tf_op jit(solution)/shard_map/all_gather | solution.py:55
  623.6 11.7 %convolution_convert_fusion = bf16[384,2048]{1,0:T(8,128)(2,1)} fusion(bf16[1408,2048]{1,0:T(8,128)(2,1)} %all-gather.17.cloned.1.call-done, bf16[384,2048]{1,0:T(8,128)(2,1)} %multiply_convert_fusion, bf16[2048,1408]{1,0:T(8,128)(2,1)} %all-gather.15.cloned.1.call-done, f32[384,1408]{1,0:T(8,128)} %fusion.12), kind=kOutput, calls=%fused_computation.14 | convolution fusion | flops 4433215488 | bytes 16842752 | tf_op jit(solution)/shard_map/dot_general | solution.py:56
  635.3 0.0 all-reduce.5.cloned.1.call-update
  635.3 18.7 %all-reduce.5.cloned.1.call-done = bf16[384,2048]{1,0:T(8,128)(2,1)} async-done(((bf16[384,2048]{1,0:T(8,128)(2,1)}), bf16[384,2048]{1,0:T(8,128)(2,1)}) %all-reduce.5.cloned.1.call-update) | async-done | bytes 1572880 | tf_op jit(solution)/shard_map/psum | solution.py:57
  654.0 4.3 add_convert_fusion
  (2 shorter events, 0.0 us)
Async XLA Ops:
  6.5 95.0 %all-gather.7.cloned.1.call-start = ((), (), s32[]{:S(2)}) async-start(), calls=%async_computation | async-start | bytes 6127616 | tf_op jit(solution)/shard_map/all_gather | solution.py:37
  7.3 204.0 %all-gather.11.cloned.1.call-start = ((), (), s32[]{:S(2)}) async-start(), calls=%async_computation.2 | async-start | bytes 6127616 | tf_op jit(solution)/shard_map/all_gather | solution.py:42
  8.0 292.9 %all-gather.9.cloned.1.call-start = ((), (), s32[]{:S(2)}) async-start(), calls=%async_computation.1 | async-start | bytes 6127616 | tf_op jit(solution)/shard_map/all_gather | solution.py:38
  8.7 322.6 %all-reduce.3.cloned.1.call-start = ((), (), s32[]{:S(2)}) async-start(), calls=%async_computation.3 | async-start | bytes 3145728 | tf_op jit(solution)/shard_map/psum | solution.py:44
  10.6 290.3 %copy-start = (bf16[384,2048]{1,0:T(8,128)(2,1)S(1)}, bf16[384,2048]{1,0:T(8,128)(2,1)}, u32[]{:S(2)}) copy-start(bf16[384,2048]{1,0:T(8,128)(2,1)} %param.10) | copy-start | bytes 4718596
  10.6 290.3 %copy-start.4 = (f32[2048]{0:T(1024)S(1)}, f32[2048]{0:T(1024)}, u32[]{:S(2)}) copy-start(f32[2048]{0:T(1024)} %param.12) | copy-start | bytes 24580
  312.1 19.2 %copy-start.1 = (bf16[384,2048]{1,0:T(8,128)(2,1)S(1)}, bf16[384,2048]{1,0:T(8,128)(2,1)}, u32[]{:S(2)}) copy-start(bf16[384,2048]{1,0:T(8,128)(2,1)} %param.11) | copy-start | bytes 4718596
  312.2 21.6 %copy-start.3 = (f32[2048]{0:T(1024)S(1)}, f32[2048]{0:T(1024)}, u32[]{:S(2)}) copy-start(f32[2048]{0:T(1024)} %param.16) | copy-start | bytes 24580
  312.2 111.7 %all-gather.13.cloned.1.call-start = ((), (), s32[]{:S(2)}) async-start(), calls=%async_computation.4 | async-start | bytes 6127616 | tf_op jit(solution)/shard_map/all_gather | solution.py:50
  312.8 201.1 %all-gather.15.cloned.1.call-start = ((), (), s32[]{:S(2)}) async-start(), calls=%async_computation.5 | async-start | bytes 6127616 | tf_op jit(solution)/shard_map/all_gather | solution.py:51
  313.3 310.2 %all-gather.17.cloned.1.call-start = ((), (), s32[]{:S(2)}) async-start(), calls=%async_computation.6 | async-start | bytes 6127616 | tf_op jit(solution)/shard_map/all_gather | solution.py:55
  314.1 340.0 %all-reduce.5.cloned.1.call-start = ((), (), s32[]{:S(2)}) async-start(), calls=%async_computation.7 | async-start | bytes 3145728 | tf_op jit(solution)/shard_map/psum | solution.py:57
  331.3 2.4 copy-start.2
Sparse Core Ops, SparseCore 0:
  10.0 91.4 all-gather.6
  104.2 106.9 all-gather.10
  213.9 86.9 all-gather.8
  312.3 19.0 all-reduce.2
  333.9 89.9 all-gather.12
  426.4 87.4 all-gather.14
  516.5 106.9 all-gather.16
  635.4 18.5 all-reduce.4
where the time goes:
time: 665 us
  waiting for transfers between devices  603 us (91%)
  matrix products  37.1 us (6%)
  between operations  13.5 us (2%)
  other arithmetic  10.8 us (2%)
    all_gather x1, waiting for transfers between devices, shards(): down_two = lax.all_gather(down_second, 'fs', axis=1, tiled=True)  110 us
    all_gather x1, waiting for transfers between devices, shards(): down_whole = lax.all_gather(down_first, 'fs', axis=1, tiled=True)  103 us
    all_gather x1, waiting for transfers between devices, shards(): lax.all_gather(gate_first, 'fs', axis=0, tiled=True)  90.9 us
    all_gather x1, waiting for transfers between devices, shards(): lax.all_gather(up_first, 'fs', axis=0, tiled=True)  89.7 us
    all_gather x1, waiting for transfers between devices, shards(): lax.all_gather(gate_second, 'fs', axis=0, tiled=True)  87.8 us
    all_gather x1, waiting for transfers between devices, shards(): lax.all_gather(up_second, 'fs', axis=0, tiled=True)  82.9 us
    psum x1, waiting for transfers between devices, shards(): lax.psum(partial_two.astype(jnp.bfloat16), 'tp').astype(jnp.float32)  18.7 us
    psum x1, waiting for transfers between devices, shards(): lax.psum(partial_value.astype(jnp.bfloat16), 'tp').astype(jnp.float32)  17 us
  transfers between devices with their start and end apart: 8, of which 8 were waited for; matrix products, arithmetic and copies ran while one was open for 3% of the time, Pallas kernels for 0%

commit v1 on v0

--- a/solution.py
+++ b/solution.py
@@ -52,7 +52,7 @@
         ),
     )
     hidden_two = (jax.nn.silu(gate_two) * up_two).astype(jnp.bfloat16)
-    down_two = lax.all_gather(down_second, "fs", axis=1, tiled=True)
+    down_two = jnp.concatenate(lax.all_gather(down_second, "fs"), axis=1)
     partial_two = jnp.dot(hidden_two, down_two, preferred_element_type=jnp.float32)
     second_sum = lax.psum(partial_two.astype(jnp.bfloat16), "tp").astype(jnp.float32)
     return (middle + 0.5 * second_sum).astype(jnp.bfloat16)

time: 665 us -> 637 us (0.958)
  waiting for transfers between devices: 603 us -> 566 us
  local copies, waits for them, and re-layouts: 0.02 us -> 8.58 us
    all_gather x1, waiting for transfers between devices: 110 us -> 76.8 us  [shards(): down_two = jnp.concatenate(lax.all_gather(down_second, 'fs'), axis=1)]
    reshape x0 -> x1, local copies, waits for them, and re-layouts: none -> 8.56 us  [shards(): down_two = jnp.concatenate(lax.all_gather(down_second, 'fs'), axis=1)]
    all_gather x1, waiting for transfers between devices: 103 us -> 110 us  [shards(): down_whole = lax.all_gather(down_first, 'fs', axis=1, tiled=True)]
    all_gather x1, waiting for transfers between devices: 89.7 us -> 83 us  [shards(): lax.all_gather(up_first, 'fs', axis=0, tiled=True)]
  transfers between devices with their start and end apart: 8 -> 8, of which waited for: 8 -> 8; matrix products, arithmetic and copies ran while one was open for 3% -> 6% of each run, Pallas kernels for 0% -> 0%
where the time goes in v1:
time: 637 us
  waiting for transfers between devices  566 us (89%)
  matrix products  37 us (6%)
  between operations  13.5 us (2%)
  other arithmetic  10.8 us (2%)
  local copies, waits for them, and re-layouts  8.58 us (1%)
    all_gather x1, waiting for transfers between devices, shards(): down_whole = lax.all_gather(down_first, 'fs', axis=1, tiled=True)  110 us
    all_gather x1, waiting for transfers between devices, shards(): lax.all_gather(gate_first, 'fs', axis=0, tiled=True)  90.3 us
    all_gather x1, waiting for transfers between devices, shards(): lax.all_gather(gate_second, 'fs', axis=0, tiled=True)  87.8 us
    all_gather x1, waiting for transfers between devices, shards(): lax.all_gather(up_second, 'fs', axis=0, tiled=True)  83.1 us
    all_gather x1, waiting for transfers between devices, shards(): lax.all_gather(up_first, 'fs', axis=0, tiled=True)  83 us
    all_gather x1, waiting for transfers between devices, shards(): down_two = jnp.concatenate(lax.all_gather(down_second, 'fs'), axis=1)  76.8 us
    psum x1, waiting for transfers between devices, shards(): lax.psum(partial_two.astype(jnp.bfloat16), 'tp').astype(jnp.float32)  19.2 us
    dot_general x2, matrix products, make_folder(): jnp.dot(normed, pieces[0], preferred_element_type=jnp.float32)  14.2 us
  transfers between devices with their start and end apart: 8, of which 8 were waited for; matrix products, arithmetic and copies ran while one was open for 6% of the time, Pallas kernels for 0%

profile of v1, /device:TPU:0, one launch (start us, length us, event | category | flops | bytes accessed | tf_op | source)
XLA Modules:
  0.0 636.8 jit_solution(6115329857536967361)
XLA Ops:
  6.5 0.0 all-gather.8.cloned.1.call-start
  6.5 0.7 all-gather.8.cloned.1.call-update
  7.3 0.0 all-gather.10.cloned.1.call-start
  7.3 0.7 all-gather.10.cloned.1.call-update
  8.0 0.0 all-gather.12.cloned.1.call-start
  8.1 0.7 all-gather.12.cloned.1.call-update
  8.7 0.0 all-gather.18.cloned.1.call-start
  8.8 0.5 all-gather.18.cloned.1.call-update
  9.3 0.0 all-reduce.3.cloned.1.call-start
  9.4 1.8 fusion.1
  11.2 0.0 copy-start
  11.2 0.0 copy-start.4
  11.2 90.3 %all-gather.8.cloned.1.call-done = bf16[2048,1408]{1,0:T(8,128)(2,1)} async-done(((bf16[128,1408]{1,0:T(8,128)(2,1)}), bf16[2048,1408]{1,0:T(8,128)(2,1)}) %all-gather.8.cloned.1.call-update) | async-done | bytes 5767184 | tf_op jit(solution)/shard_map/all_gather | solution.py:37
  101.5 7.2 %fusion.8 = f32[384,1408]{1,0:T(8,128)} fusion(bf16[2048,1408]{1,0:T(8,128)(2,1)} %all-gather.8.cloned.1.call-done, bf16[384,2048]{1,0:T(8,128)(2,1)} %param.10, f32[2048]{0:T(1024)} %param.12, f32[384]{0:T(512)S(1)} %add_rsqrt_fusion.1), kind=kOutput, calls=%fused_computation.16 | convolution fusion | flops 2217738240 | bytes 9512448 | tf_op jit(solution)/shard_map/dot_general | solution.py:16
  108.7 83.0 %all-gather.10.cloned.1.call-done = bf16[2048,1408]{1,0:T(8,128)(2,1)} async-done(((bf16[128,1408]{1,0:T(8,128)(2,1)}), bf16[2048,1408]{1,0:T(8,128)(2,1)}) %all-gather.10.cloned.1.call-update) | async-done | bytes 5767184 | tf_op jit(solution)/shard_map/all_gather | solution.py:38
  191.7 109.7 %all-gather.12.cloned.1.call-done = bf16[1408,2048]{1,0:T(8,128)(2,1)} async-done(((bf16[1408,128]{1,0:T(8,128)(2,1)}), bf16[1408,2048]{1,0:T(8,128)(2,1)}) %all-gather.12.cloned.1.call-update) | async-done | bytes 5767184 | tf_op jit(solution)/shard_map/all_gather | solution.py:42
  301.4 0.0 copy-done
  301.4 0.0 copy-done.4
  301.4 11.2 %convolution_convert_fusion.1 = bf16[384,2048]{1,0:T(8,128)(2,1)} fusion(bf16[1408,2048]{1,0:T(8,128)(2,1)} %all-gather.12.cloned.1.call-done, bf16[2048,1408]{1,0:T(8,128)(2,1)} %all-gather.10.cloned.1.call-done, f32[384,1408]{1,0:T(8,128)} %fusion.8, bf16[384,2048]{1,0:T(8,128)(2,1)S(1)} %copy-done, f32[2048]{0:T(1024)S(1)} %copy-done.4, ...), kind=kOutput, calls=%fused_computation.15 | convolution fusion | flops 4436361216 | bytes 16852480 | tf_op jit(solution)/shard_map/dot_general | solution.py:43
  312.6 0.0 all-reduce.3.cloned.1.call-update
  312.6 0.0 all-gather.14.cloned.1.call-start
  312.7 0.5 all-gather.14.cloned.1.call-update
  313.2 0.0 all-gather.16.cloned.1.call-start
  313.3 0.7 all-gather.16.cloned.1.call-update
  314.0 0.2 all-reduce.5.cloned.1.call-start
  314.2 76.8 %all-gather.18.cloned.1.call-done = bf16[22528,128]{1,0:T(8,128)(2,1)} async-done(((bf16[1408,128]{1,0:T(8,128)(2,1)}), bf16[22528,128]{1,0:T(8,128)(2,1)}) %all-gather.18.cloned.1.call-update) | async-done | bytes 5767184 | tf_op jit(solution)/shard_map/all_gather | solution.py:55
  391.0 0.0 copy-start.1
  391.0 8.6 %copy.11 = bf16[1408,16,128]{0,2,1:T(8,128)(2,1)} copy(bf16[1408,16,128]{2,0,1:T(8,128)(2,1)} %bitcast.12) | data formatting | bytes 11534336 | tf_op jit(solution)/shard_map/reshape | solution.py:55
  399.5 0.0 copy-start.3
  399.5 12.7 %all-reduce.3.cloned.1.call-done = bf16[384,2048]{1,0:T(8,128)(2,1)} async-done(((bf16[384,2048]{1,0:T(8,128)(2,1)}), bf16[384,2048]{1,0:T(8,128)(2,1)}) %all-reduce.3.cloned.1.call-update) | async-done | bytes 1572880 | tf_op jit(solution)/shard_map/psum | solution.py:44
  412.2 0.0 copy-done.1
  412.2 0.0 copy-start.2
  412.2 2.4 multiply_reduce_fusion
  414.6 0.0 copy-done.3
  414.7 0.0 copy-done.2
  414.7 2.2 multiply_convert_fusion
  416.9 87.8 %all-gather.14.cloned.1.call-done = bf16[2048,1408]{1,0:T(8,128)(2,1)} async-done(((bf16[128,1408]{1,0:T(8,128)(2,1)}), bf16[2048,1408]{1,0:T(8,128)(2,1)}) %all-gather.14.cloned.1.call-update) | async-done | bytes 5767184 | tf_op jit(solution)/shard_map/all_gather | solution.py:50
  504.7 7.1 %fusion.12 = f32[384,1408]{1,0:T(8,128)} fusion(bf16[384,2048]{1,0:T(8,128)(2,1)} %multiply_convert_fusion, bf16[2048,1408]{1,0:T(8,128)(2,1)} %all-gather.14.cloned.1.call-done), kind=kOutput, calls=%fused_computation.21 | convolution fusion | flops 2214592512 | bytes 9502720 | tf_op jit(solution)/shard_map/dot_general | solution.py:16
  511.8 83.1 %all-gather.16.cloned.1.call-done = bf16[2048,1408]{1,0:T(8,128)(2,1)} async-done(((bf16[128,1408]{1,0:T(8,128)(2,1)}), bf16[2048,1408]{1,0:T(8,128)(2,1)}) %all-gather.16.cloned.1.call-update) | async-done | bytes 5767184 | tf_op jit(solution)/shard_map/all_gather | solution.py:51
  594.9 11.6 %convolution_convert_fusion = bf16[384,2048]{1,0:T(8,128)(2,1)} fusion(bf16[1408,2048]{0,1:T(8,128)(2,1)} %bitcast.13, bf16[384,2048]{1,0:T(8,128)(2,1)} %multiply_convert_fusion, bf16[2048,1408]{1,0:T(8,128)(2,1)} %all-gather.16.cloned.1.call-done, f32[384,1408]{1,0:T(8,128)} %fusion.12), kind=kOutput, calls=%fused_computation.14 | convolution fusion | flops 4433215488 | bytes 16842752 | tf_op jit(solution)/shard_map/dot_general | solution.py:56
  606.5 0.0 all-reduce.5.cloned.1.call-update
  606.5 19.2 %all-reduce.5.cloned.1.call-done = bf16[384,2048]{1,0:T(8,128)(2,1)} async-done(((bf16[384,2048]{1,0:T(8,128)(2,1)}), bf16[384,2048]{1,0:T(8,128)(2,1)}) %all-reduce.5.cloned.1.call-update) | async-done | bytes 1572880 | tf_op jit(solution)/shard_map/psum | solution.py:57
  625.7 4.3 add_convert_fusion
  (2 shorter events, 0.0 us)
Async XLA Ops:
  6.5 95.0 %all-gather.8.cloned.1.call-start = ((), (), s32[]{:S(2)}) async-start(), calls=%async_computation | async-start | bytes 6127616 | tf_op jit(solution)/shard_map/all_gather | solution.py:37
  7.3 184.4 %all-gather.10.cloned.1.call-start = ((), (), s32[]{:S(2)}) async-start(), calls=%async_computation.1 | async-start | bytes 6127616 | tf_op jit(solution)/shard_map/all_gather | solution.py:38
  8.0 293.4 %all-gather.12.cloned.1.call-start = ((), (), s32[]{:S(2)}) async-start(), calls=%async_computation.2 | async-start | bytes 6127616 | tf_op jit(solution)/shard_map/all_gather | solution.py:42
  8.7 382.2 %all-gather.18.cloned.1.call-start = ((), (), s32[]{:S(2)}) async-start(), calls=%async_computation.7 | async-start | bytes 6127616 | tf_op jit(solution)/shard_map/all_gather | solution.py:55
  9.3 402.9 %all-reduce.3.cloned.1.call-start = ((), (), s32[]{:S(2)}) async-start(), calls=%async_computation.3 | async-start | bytes 3145728 | tf_op jit(solution)/shard_map/psum | solution.py:44
  11.2 290.2 %copy-start = (bf16[384,2048]{1,0:T(8,128)(2,1)S(1)}, bf16[384,2048]{1,0:T(8,128)(2,1)}, u32[]{:S(2)}) copy-start(bf16[384,2048]{1,0:T(8,128)(2,1)} %param.10) | copy-start | bytes 4718596
  11.2 290.2 %copy-start.4 = (f32[2048]{0:T(1024)S(1)}, f32[2048]{0:T(1024)}, u32[]{:S(2)}) copy-start(f32[2048]{0:T(1024)} %param.12) | copy-start | bytes 24580
  312.6 192.1 %all-gather.14.cloned.1.call-start = ((), (), s32[]{:S(2)}) async-start(), calls=%async_computation.4 | async-start | bytes 6127616 | tf_op jit(solution)/shard_map/all_gather | solution.py:50
  313.2 281.7 %all-gather.16.cloned.1.call-start = ((), (), s32[]{:S(2)}) async-start(), calls=%async_computation.5 | async-start | bytes 6127616 | tf_op jit(solution)/shard_map/all_gather | solution.py:51
  314.0 311.7 %all-reduce.5.cloned.1.call-start = ((), (), s32[]{:S(2)}) async-start(), calls=%async_computation.6 | async-start | bytes 3145728 | tf_op jit(solution)/shard_map/psum | solution.py:57
  391.0 21.3 %copy-start.1 = (bf16[384,2048]{1,0:T(8,128)(2,1)S(1)}, bf16[384,2048]{1,0:T(8,128)(2,1)}, u32[]{:S(2)}) copy-start(bf16[384,2048]{1,0:T(8,128)(2,1)} %param.11) | copy-start | bytes 4718596
  399.5 15.1 %copy-start.3 = (f32[2048]{0:T(1024)S(1)}, f32[2048]{0:T(1024)}, u32[]{:S(2)}) copy-start(f32[2048]{0:T(1024)} %param.16) | copy-start | bytes 24580
  412.2 2.4 copy-start.2
Sparse Core Ops, SparseCore 0:
  10.0 91.4 all-gather.7
  104.2 87.4 all-gather.9
  194.4 106.9 all-gather.11
  303.9 86.9 all-gather.17
  393.1 19.0 all-reduce.2
  414.8 89.9 all-gather.13
  507.4 87.4 all-gather.15
  606.6 19.0 all-reduce.4
